TPU v7x, 128 devices: a whole 4x4x4 slice. The times are simulated.
128 devices in a mesh: rep: 2 (over z_hi), fs: 32 (over z_lo, y, x), tp: 2 (over core).
Axes of the slice: x: 4, y: 4, z: 4 (z_hi: 2, z_lo: 2; z = z_hi * 2 + z_lo), core: 2. Of those that a mesh axis runs over, the one named last changes fastest.
Arguments:
- sequence: bfloat16 [64, 768, 2048], P(('rep', 'fs'), None, 'tp'), may hold values from -6 to 6
- mix_gain: float32 [2048], replicated, may hold values from 0.1 to 1.9
- ffn_gain: float32 [2048], replicated, may hold values from 0.1 to 1.9
- proj_outer: float32 [2048, 2048], P(None, ('tp', 'fs')), may hold values from -0.125 to 0.125
- proj_inner: float32 [2048, 2048], P(None, ('tp', 'fs')), may hold values from -0.125 to 0.125
- proj_value: float32 [2048, 2048], P(None, ('tp', 'fs')), may hold values from -0.125 to 0.125
- proj_scales: float32 [3, 2048], P(None, 'tp'), may hold values from 0.5 to 2
- taps: float32 [3, 2048], P(None, 'tp'), may hold values from -3 to 3
- mix_out: float32 [2048, 2048], P('tp', 'fs'), may hold values from -0.125 to 0.125
- mix_out_scale: float32 [2048], P('fs'), may hold values from 0.5 to 2
- ffn_gate: float32 [2048, 2816], P(None, ('tp', 'fs')), may hold values from -0.125 to 0.125
- ffn_up: float32 [2048, 2816], P(None, ('tp', 'fs')), may hold values from -0.125 to 0.125
- ffn_scales: float32 [2, 2816], P(None, 'tp'), may hold values from 0.5 to 2
- ffn_down: float32 [2816, 2048], P('tp', 'fs'), may hold values from -0.109375 to 0.109375
- down_scale: float32 [2048], P('fs'), may hold values from 0.5 to 2
Outputs:
- layer_out: bfloat16 [64, 768, 2048], P(('rep', 'fs'), None, 'tp')
All inputs are finite; a program needn't handle non-finite values.
Results may differ from a plain program's by a relative error of at most 0.013.
Values may be sent and summed in bfloat16 or wider, within the bound.
A program may use at most 128 MiB of HBM per device.

v0:
```python
import jax
import jax.numpy as jnp
from jax import lax
from jax.sharding import PartitionSpec as P

eps = 1e-06


def gather_turned(arrays, axis, dims):
    turned = [jnp.moveaxis(a, dim, 0) for a, dim in zip(arrays, dims)]
    both = jnp.concatenate([t.reshape(len(t), -1) for t in turned], axis=1)
    out, at, outs = (lax.all_gather(both, axis, axis=0, tiled=True), 0, [])
    for t, dim in zip(turned, dims):
        share = out[:, at : at + t[0].size].reshape(-1, *t.shape[1:])
        outs.append(jnp.moveaxis(share, 0, dim))
        at += t[0].size
    return tuple(outs)


def in_blocks(array, dim, devices):
    lengths = array.shape
    blocks = array.reshape(*lengths[:dim], devices, lengths[dim] // devices, *lengths[dim + 1 :])
    return jnp.moveaxis(blocks, dim, 0)


def sent_and_summed(array, axis, dim):
    blocks = in_blocks(array, dim, lax.axis_size(axis))
    arrived = lax.all_to_all(blocks, axis, split_axis=0, concat_axis=0, tiled=True)
    return arrived.astype(jnp.float32).sum(axis=0)


def rms_rows(rows, gain):
    values = rows.astype(jnp.float32)
    scaled = values * lax.rsqrt(jnp.mean(values * values, axis=-1, keepdims=True) + eps)
    return (scaled * gain).astype(jnp.bfloat16)


def body(
    sequence,
    mix_gain,
    ffn_gain,
    proj_outer,
    proj_inner,
    proj_value,
    proj_scales,
    taps,
    mix_out,
    mix_out_scale,
    ffn_gate,
    ffn_up,
    ffn_scales,
    ffn_down,
    down_scale,
):
    local = sequence[0]
    full_rows = lax.all_gather(local, "tp", axis=1, tiled=True)
    normed = rms_rows(full_rows, mix_gain)
    out_scales = gather_turned((mix_out_scale, down_scale), "fs", (0, 0))
    w_outer = proj_outer.astype(jnp.bfloat16)
    w_inner = proj_inner.astype(jnp.bfloat16)
    w_value = proj_value.astype(jnp.bfloat16)
    whole_outer, whole_inner, whole_value = gather_turned(
        (w_outer, w_inner, w_value), "fs", (1, 1, 1)
    )
    outer = jnp.dot(normed, whole_outer, preferred_element_type=jnp.float32)
    inner = jnp.dot(normed, whole_inner, preferred_element_type=jnp.float32)
    value = jnp.dot(normed, whole_value, preferred_element_type=jnp.float32)
    carried = inner * proj_scales[1] * (value * proj_scales[2])
    length = carried.shape[0]
    back_one = jnp.pad(carried, ((1, 0), (0, 0)))[:length]
    back_two = jnp.pad(carried, ((2, 0), (0, 0)))[:length]
    conv = taps[0] * back_two + taps[1] * back_one + taps[2] * carried
    gated = (outer * proj_scales[0] * conv).astype(jnp.bfloat16)
    scale = out_scales[0]
    mixer_terms = (
        jnp.dot(
            gated,
            lax.all_gather(mix_out.astype(jnp.bfloat16), "fs", axis=1, tiled=True),
            preferred_element_type=jnp.float32,
        )
        * scale
    )
    mix = sent_and_summed(mixer_terms.astype(jnp.bfloat16), "tp", 1)
    after = (local.astype(jnp.float32) + mix).astype(jnp.bfloat16)
    after_rows = lax.all_gather(after, "tp", axis=1, tiled=True)
    normed2 = rms_rows(after_rows, ffn_gain)
    w_gate = ffn_gate.astype(jnp.bfloat16)
    w_up = ffn_up.astype(jnp.bfloat16)
    whole_gate, whole_up = gather_turned((w_gate, w_up), "fs", (1, 1))
    gate = jnp.dot(normed2, whole_gate, preferred_element_type=jnp.float32)
    up = jnp.dot(normed2, whole_up, preferred_element_type=jnp.float32)
    hidden = (jax.nn.silu(gate * ffn_scales[0]) * (up * ffn_scales[1])).astype(jnp.bfloat16)
    scale = out_scales[1]
    ffn_terms = (
        jnp.dot(
            hidden,
            lax.all_gather(ffn_down.astype(jnp.bfloat16), "fs", axis=1, tiled=True),
            preferred_element_type=jnp.float32,
        )
        * scale
    )
    ffn = sent_and_summed(ffn_terms.astype(jnp.bfloat16), "tp", 1)
    result = (after.astype(jnp.float32) + ffn).astype(jnp.bfloat16)
    return result[None]


def solution(mesh):
    in_specs = (
        P(("rep", "fs"), None, "tp"),
        P(),
        P(),
        P(None, ("tp", "fs")),
        P(None, ("tp", "fs")),
        P(None, ("tp", "fs")),
        P(None, "tp"),
        P(None, "tp"),
        P("tp", "fs"),
        P("fs"),
        P(None, ("tp", "fs")),
        P(None, ("tp", "fs")),
        P(None, "tp"),
        P("tp", "fs"),
        P("fs"),
    )
    out_specs = P(("rep", "fs"), None, "tp")
    return jax.shard_map(body, mesh=mesh, in_specs=in_specs, out_specs=out_specs, check_vma=False)
```

profile of v0, /device:TPU:1, one launch (start us, length us, event | category | flops | bytes accessed | tf_op | source)
XLA Modules:
  0.0 752.1 jit_solution(7647889185761469245)
XLA Ops:
  6.5 0.0 copy-start.6
  6.5 0.0 copy-start.4
  6.5 0.0 copy-start.3
  6.5 0.0 copy-start.8
  6.6 0.0 copy-start.9
  6.6 0.0 all-gather.18.cloned.1.call-start
  6.6 0.7 all-gather.18.cloned.1.call-update
  7.3 0.0 all-gather.10.cloned.1.call-start
  7.3 1.0 convert_bitcast_fusion.5
  8.3 1.1 convert_bitcast_fusion.3
  9.4 0.8 pad_maximum_fusion
  10.2 0.0 all-gather.10.cloned.1.call-update
  10.2 0.0 copy-start.12
  10.2 0.0 all-gather.12.cloned.1.call-start
  10.2 0.0 copy-done.6
  10.3 0.7 convert_element_type.82
  10.9 0.0 all-gather.12.cloned.1.call-update
  10.9 0.0 all-gather.20.cloned.1.call-start
  11.0 0.0 copy-done.4
  11.0 0.0 copy-done.3
  11.1 0.8 maximum_bitcast_fusion
  11.9 0.0 all-gather.20.cloned.1.call-update
  11.9 0.0 all-gather.14.cloned.1.call-start
  11.9 0.0 copy-done.11
  12.0 0.0 copy-done.10
  12.0 72.3 %all-gather.1 = f32[32,64,2]{1,2,0:T(2,128)S(1)} all-gather(f32[1,64,2]{1,2,0:T(2,128)S(1)} %maximum_bitcast_fusion.1), channel_id=1, replica_groups=mesh['rep'=2,'fs'=32,'tp'=2] {'fs'}, dimensions={0}, use_global_device_ids=true | all-gather | bytes 16896 | tf_op jit(solution)/shard_map/all_gather | solution.py:12
  84.3 0.1 reshape.42
  84.4 0.0 copy-done.8
  84.4 0.0 copy-done.9
  84.5 0.0 all-gather.18.cloned.1.call-done
  84.5 2.6 fusion.3
  87.1 0.0 copy-start.2
  87.1 100.5 %all-gather.10.cloned.1.call-done = bf16[1024,6144]{1,0:T(8,128)(2,1)} async-done(((bf16[32,6144]{1,0:T(8,128)(2,1)}), bf16[1024,6144]{1,0:T(8,128)(2,1)}) %all-gather.10.cloned.1.call-update) | async-done | bytes 12582928 | tf_op jit(solution)/shard_map/all_gather | solution.py:12
  187.7 0.0 copy-done.12
  187.7 6.2 fusion.10
  193.9 0.0 copy-done.2
  193.9 7.3 multiply_multiply_fusion
  201.2 140.5 %all-gather.12.cloned.1.call-done = bf16[1024,2048]{0,1:T(8,128)(2,1)} async-done(((bf16[1024,64]{0,1:T(8,128)(2,1)}), bf16[1024,2048]{0,1:T(8,128)(2,1)}) %all-gather.12.cloned.1.call-update) | async-done | bytes 4194320 | tf_op jit(solution)/shard_map/all_gather | solution.py:78
  341.7 15.4 %multiply_convert_fusion.1 = bf16[768,2048]{1,0:T(8,128)(2,1)} fusion(bf16[1024,2048]{0,1:T(8,128)(2,1)} %all-gather.12.cloned.1.call-done, f32[2048]{0:T(1024)S(1)} %bitcast.70, f32[768,1024]{1,0:T(8,128)} %multiply_multiply_fusion, bf16[1024,6144]{1,0:T(8,128)(2,1)} %all-gather.10.cloned.1.call-done, f32[1024]{0:T(1024)S(1)} %bitcast.73, ...), kind=kOutput, calls=%fused_computation.13 | convolution fusion | flops 6458179584 | bytes 17861632 | tf_op jit(solution)/shard_map/dot_general | solution.py:76
  357.1 2.3 copy.25
  359.3 26.6 %all_to_all.10 = bf16[2,768,1024]{2,1,0:T(8,128)(2,1)S(1)} all-to-all(bf16[2,768,1024]{2,1,0:T(8,128)(2,1)S(1)} %bitcast.65), channel_id=1, replica_groups=mesh['rep'=2,'fs'=32,'tp'=2] {'tp'}, dimensions={0} | all-to-all | bytes 6291456 | tf_op jit(solution)/shard_map/all_to_all | solution.py:28
  385.9 0.7 convert_reduce_fusion.1
  386.6 0.7 copy-done
  387.3 1.7 fusion.26
  389.0 0.0 all-gather.14.cloned.1.call-update
  389.1 0.0 all-gather.16.cloned.1.call-start
  389.1 0.0 copy-done.5
  389.1 0.7 convert_element_type.94
  389.8 0.0 all-gather.16.cloned.1.call-update
  389.8 0.0 copy-done.7
  389.9 0.0 copy-start.13
  389.9 130.2 %all-gather.20.cloned.1.call-done = bf16[32,44,4096]{2,1,0:T(8,128)(2,1)} async-done(((bf16[1,44,4096]{2,1,0:T(8,128)(2,1)}), bf16[32,44,4096]{2,1,0:T(8,128)(2,1)}) %all-gather.20.cloned.1.call-update) | async-done | bytes 11534352 | tf_op jit(solution)/shard_map/all_gather | solution.py:12
  520.1 14.3 %reshape.44 = bf16[1408,4096]{1,0:T(8,128)(2,1)} reshape(bf16[32,44,4096]{2,1,0:T(8,128)(2,1)} %all-gather.20.cloned.1.call-done) | data formatting | bytes 23068672
  534.4 18.9 %all-gather.14.cloned.1.call-done = bf16[768,2048]{1,0:T(8,128)(2,1)} async-done(((bf16[768,1024]{1,0:T(8,128)(2,1)}), bf16[768,2048]{1,0:T(8,128)(2,1)}) %all-gather.14.cloned.1.call-update) | async-done | bytes 3145744 | tf_op jit(solution)/shard_map/all_gather | solution.py:85
  553.3 2.6 fusion
  555.9 0.0 copy-done.13
  555.9 9.9 %fusion.6 = f32[768,1408]{1,0:T(8,128)} fusion(bf16[1408,4096]{1,0:T(8,128)(2,1)} %reshape.44, bf16[768,2048]{1,0:T(8,128)(2,1)} %all-gather.14.cloned.1.call-done, f32[2048]{0:T(1024)S(1)} %copy-done.13, f32[768]{0:T(1024)S(1)} %add_rsqrt_fusion), kind=kOutput, calls=%fused_computation.14 | convolution fusion | flops 4435476480 | bytes 13249536 | tf_op jit(solution)/shard_map/dot_general | solution.py:91
  565.8 130.3 %all-gather.16.cloned.1.call-done = bf16[1408,2048]{0,1:T(8,128)(2,1)} async-done(((bf16[1408,64]{0,1:T(8,128)(2,1)}), bf16[1408,2048]{0,1:T(8,128)(2,1)}) %all-gather.16.cloned.1.call-update) | async-done | bytes 5767184 | tf_op jit(solution)/shard_map/all_gather | solution.py:97
  696.1 17.4 %multiply_convert_fusion = bf16[768,2048]{1,0:T(8,128)(2,1)} fusion(bf16[1408,2048]{0,1:T(8,128)(2,1)} %all-gather.16.cloned.1.call-done, f32[2048]{0:T(1024)S(1)} %bitcast.69, f32[768,1408]{1,0:T(8,128)} %fusion.6, bf16[1408,4096]{1,0:T(8,128)(2,1)} %reshape.44, f32[1408]{0:T(1024)S(1)} %get-tuple-element.6, f32[1408]{0:T(1024)S(1)} %get-tuple-element.5, ...), kind=kOutput, calls=%fused_computation.11 | convolution fusion | flops 8876457984 | bytes 22181888 | tf_op jit(solution)/shard_map/dot_general | solution.py:95
  713.5 2.3 copy.24
  715.8 26.0 %all_to_all.11 = bf16[2,768,1024]{2,1,0:T(8,128)(2,1)S(1)} all-to-all(bf16[2,768,1024]{2,1,0:T(8,128)(2,1)S(1)} %bitcast.66), channel_id=1, replica_groups=mesh['rep'=2,'fs'=32,'tp'=2] {'tp'}, dimensions={0} | all-to-all | bytes 6291456 | tf_op jit(solution)/shard_map/all_to_all | solution.py:28
  741.8 0.7 convert_reduce_fusion
  742.5 0.7 copy-done.1
  743.2 2.1 fusion.27
  (15 shorter events, 0.2 us)
Async XLA Ops:
  6.5 3.7 copy-start.6
  6.5 4.4 copy-start.4
  6.5 4.5 copy-start.3
  6.5 5.4 copy-start.11
  6.5 5.4 copy-start.10
  6.5 77.8 %copy-start.8 = (f32[3,1024]{1,0:T(4,128)S(1)}, f32[3,1024]{1,0:T(4,128)}, u32[]{:S(2)}) copy-start(f32[3,1024]{1,0:T(4,128)} %param.21) | copy-start | bytes 36868
  6.6 77.9 %copy-start.9 = (f32[3,1024]{1,0:T(4,128)S(1)}, f32[3,1024]{1,0:T(4,128)}, u32[]{:S(2)}) copy-start(f32[3,1024]{1,0:T(4,128)} %param.22) | copy-start | bytes 36868
  6.6 77.9 %all-gather.18.cloned.1.call-start = ((), (), s32[]{:S(2)}) async-start(), calls=%async_computation.6 | async-start | bytes 4718592 | tf_op jit(solution)/shard_map/all_gather | solution.py:56
  7.3 180.4 %all-gather.10.cloned.1.call-start = ((), (), s32[]{:S(2)}) async-start(), calls=%async_computation.2 | async-start | bytes 12976128 | tf_op jit(solution)/shard_map/all_gather | solution.py:12
  10.2 177.5 %copy-start.12 = (f32[2048]{0:T(1024)S(1)}, f32[2048]{0:T(1024)}, u32[]{:S(2)}) copy-start(f32[2048]{0:T(1024)} %param.16) | copy-start | bytes 24580
  10.2 331.5 %all-gather.12.cloned.1.call-start = ((), (), s32[]{:S(2)}) async-start(), calls=%async_computation.3 | async-start | bytes 4325376 | tf_op jit(solution)/shard_map/all_gather | solution.py:78
  10.9 509.2 %all-gather.20.cloned.1.call-start = ((), (), s32[]{:S(2)}) async-start(), calls=%async_computation.7 | async-start | bytes 12976128 | tf_op jit(solution)/shard_map/all_gather | solution.py:12
  11.9 541.5 %all-gather.14.cloned.1.call-start = ((), (), s32[]{:S(2)}) async-start(), calls=%async_computation.4 | async-start | bytes 4718592 | tf_op jit(solution)/shard_map/all_gather | solution.py:85
  87.1 106.8 %copy-start.2 = (bf16[1,768,2048]{2,1,0:T(8,128)(2,1)S(1)}, bf16[1,768,2048]{2,1,0:T(8,128)(2,1)}, u32[]{:S(2)}) copy-start(bf16[1,768,2048]{2,1,0:T(8,128)(2,1)} %all-gather.18.cloned.1.call-done) | copy-start | bytes 9437188
  385.9 1.4 copy-start
  387.3 1.8 copy-start.5
  387.3 2.5 copy-start.7
  389.1 307.1 %all-gather.16.cloned.1.call-start = ((), (), s32[]{:S(2)}) async-start(), calls=%async_computation.5 | async-start | bytes 5947392 | tf_op jit(solution)/shard_map/all_gather | solution.py:97
  389.9 166.0 %copy-start.13 = (f32[2048]{0:T(1024)S(1)}, f32[2048]{0:T(1024)}, u32[]{:S(2)}) copy-start(f32[2048]{0:T(1024)} %param.17) | copy-start | bytes 24580
  741.8 1.4 copy-start.1
Sparse Core Ops, SparseCore 0:
  9.0 18.4 all-gather.17
  29.2 158.4 all-gather.9
  189.3 152.3 all-gather.11
  343.2 176.8 all-gather.19
  521.6 31.6 all-gather.13
  554.8 141.2 all-gather.15
where the time goes:
time: 753 us; the launch traced here: 752 us
  waiting for transfers between devices  521 us (69%)
  blocking collectives  125 us (17%)
  matrix products  56.2 us (7%)
  local copies, waits for them, and re-layouts  20.5 us (3%)
  other arithmetic  15.4 us (2%)
  between operations  13.7 us (2%)
    all_gather x2, waiting for transfers between devices, gather_turned(): out, at, outs = (lax.all_gather(both, axis, axis=0, tiled=True), 0, [])  231 us
    all_gather x1, waiting for transfers between devices, body(): lax.all_gather(mix_out.astype(jnp.bfloat16), 'fs', axis=1, tiled=True)  140 us
    all_gather x1, waiting for transfers between devices, body(): lax.all_gather(ffn_down.astype(jnp.bfloat16), 'fs', axis=1, tiled=True)  130 us
    all_gather x1, blocking collectives, gather_turned(): out, at, outs = (lax.all_gather(both, axis, axis=0, tiled=True), 0, [])  72.3 us
    all_to_all x2, blocking collectives, sent_and_summed(): lax.all_to_all(blocks, axis, split_axis=0, concat_axis=0, tiled=True)  52.5 us
    all_gather x1, waiting for transfers between devices, body(): after_rows = lax.all_gather(after, 'tp', axis=1, tiled=True)  18.9 us
    dot_general x1, matrix products, body(): jnp.dot(hidden, lax.all_gather(ffn_down.astype(jnp.bfloat16), 'fs', axis=...  17.4 us
    unnamed x30, local copies, waits for them, and re-layouts  15.9 us
  transfers between devices with their start and end apart: 6, of which 5 were waited for; matrix products, arithmetic and copies ran while one was open for 9% of the time, Pallas kernels for 0%

commit v1 on v0

--- a/solution.py
+++ b/solution.py
@@ -52,6 +52,13 @@
     ffn_down,
     down_scale,
 ):
+
+    def group_wall(xin):
+        return jnp.concatenate(
+            jax.lax.all_to_all(jnp.stack(jax.lax.axis_size("fs") * [xin], axis=0), "fs", 0, 0),
+            axis=1,
+        )
+
     local = sequence[0]
     full_rows = lax.all_gather(local, "tp", axis=1, tiled=True)
     normed = rms_rows(full_rows, mix_gain)
@@ -73,11 +80,7 @@
     gated = (outer * proj_scales[0] * conv).astype(jnp.bfloat16)
     scale = out_scales[0]
     mixer_terms = (
-        jnp.dot(
-            gated,
-            lax.all_gather(mix_out.astype(jnp.bfloat16), "fs", axis=1, tiled=True),
-            preferred_element_type=jnp.float32,
-        )
+        jnp.dot(gated, group_wall(mix_out.astype(jnp.bfloat16)), preferred_element_type=jnp.float32)
         * scale
     )
     mix = sent_and_summed(mixer_terms.astype(jnp.bfloat16), "tp", 1)

time: 753 us -> 624 us (0.83)
  waiting for transfers between devices: 521 us -> 327 us
  blocking collectives: 125 us -> 180 us
  starting transfers between devices: 0.24 us -> 9.65 us
    all_gather x1 -> x0, waiting for transfers between devices: 140 us -> none  [body(): lax.all_gather(mix_out.astype(jnp.bfloat16), 'fs', axis=1, tiled=True)]
    all_gather x1, blocking collectives: 72.3 us -> 131 us  [gather_turned(): out, at, outs = (lax.all_gather(both, axis, axis=0, tiled=True), 0, [])]
    all_gather x2, waiting for transfers between devices: 231 us -> 177 us  [gather_turned(): out, at, outs = (lax.all_gather(both, axis, axis=0, tiled=True), 0, [])]
    all_to_all x0 -> x1, starting transfers between devices: none -> 9.49 us  [group_wall(): jax.lax.all_to_all(jnp.stack(jax.lax.axis_size('fs') * [xin], axis=0), 'f...]
  transfers between devices with their start and end apart: 6 -> 6, of which waited for: 5 -> 4; matrix products, arithmetic and copies ran while one was open for 9% -> 11% of each run, Pallas kernels for 0% -> 0%
where the time goes in v1:
time: 624 us; the launch traced here: 623 us
  waiting for transfers between devices  327 us (52%)
  blocking collectives  180 us (29%)
  matrix products  56.1 us (9%)
  local copies, waits for them, and re-layouts  22.9 us (4%)
  other arithmetic  14.7 us (2%)
  between operations  13.4 us (2%)
  starting transfers between devices  9.65 us (2%)
    all_gather x2, waiting for transfers between devices, gather_turned(): out, at, outs = (lax.all_gather(both, axis, axis=0, tiled=True), 0, [])  177 us
    all_gather x1, blocking collectives, gather_turned(): out, at, outs = (lax.all_gather(both, axis, axis=0, tiled=True), 0, [])  131 us
    all_gather x1, waiting for transfers between devices, body(): lax.all_gather(ffn_down.astype(jnp.bfloat16), 'fs', axis=1, tiled=True)  130 us
    all_to_all x2, blocking collectives, sent_and_summed(): lax.all_to_all(blocks, axis, split_axis=0, concat_axis=0, tiled=True)  48.5 us
    all_gather x1, waiting for transfers between devices, body(): after_rows = lax.all_gather(after, 'tp', axis=1, tiled=True)  19 us
    dot_general x1, matrix products, body(): jnp.dot(hidden, lax.all_gather(ffn_down.astype(jnp.bfloat16), 'fs', axis=...  17.4 us
    unnamed x30, local copies, waits for them, and re-layouts  15.9 us
    dot_general x1, matrix products, body(): jnp.dot(gated, group_wall(mix_out.astype(jnp.bfloat16)), preferred_elemen...  15.2 us
  transfers between devices with their start and end apart: 6, of which 4 were waited for; matrix products, arithmetic and copies ran while one was open for 11% of the time, Pallas kernels for 0%

profile of v1, /device:TPU:1, one launch (start us, length us, event | category | flops | bytes accessed | tf_op | source)
XLA Modules:
  0.0 623.4 jit_solution(616493204678986122)
XLA Ops:
  6.5 0.0 copy-start.4
  6.5 0.0 copy-start.3
  6.5 0.0 copy-start.6
  6.5 0.0 all-gather.15.cloned.1.call-start
  6.5 0.7 all-gather.15.cloned.1.call-update
  7.3 0.0 all-gather.9.cloned.1.call-start
  7.3 1.0 convert_bitcast_fusion.5
  8.3 1.1 convert_bitcast_fusion.3
  9.3 0.8 pad_maximum_fusion
  10.1 0.0 all-gather.9.cloned.1.call-update
  10.1 0.0 all-gather.17.cloned.1.call-start
  10.2 0.0 copy-done.4
  10.2 0.0 copy-done.3
  10.3 0.8 maximum_bitcast_fusion
  11.1 0.0 all-gather.17.cloned.1.call-update
  11.1 0.0 copy-done.6
  11.1 2.5 stack.2
  13.6 0.0 copy-start.10
  13.6 0.0 copy-start.11
  13.6 0.0 copy-start.8
  13.6 9.5 %all-to-all-start = ((bf16[32,1024,64]{1,2,0:T(8,128)(2,1)}), bf16[32,1024,64]{1,2,0:T(8,128)(2,1)}, u32[]{:S(2)}, u32[]{:S(2)}) async-start(bf16[32,1024,64]{1,2,0:T(8,128)(2,1)} %stack.2), calls=%async_computation | async-start | bytes 8388608 | tf_op jit(solution)/shard_map/all_to_all | solution.py:58
  23.1 0.0 copy-start.12
  23.1 0.0 all-gather.11.cloned.1.call-start
  23.2 0.0 copy-done.10
  23.2 0.0 copy-done.11
  23.2 131.0 %all-gather.1 = f32[32,64,2]{1,2,0:T(2,128)S(1)} all-gather(f32[1,64,2]{1,2,0:T(2,128)S(1)} %maximum_bitcast_fusion.1), channel_id=1, replica_groups=mesh['rep'=2,'fs'=32,'tp'=2] {'fs'}, dimensions={0}, use_global_device_ids=true | all-gather | bytes 16896 | tf_op jit(solution)/shard_map/all_gather | solution.py:12
  154.2 0.1 reshape.52
  154.3 0.0 copy-done.8
  154.4 0.0 copy-done.9
  154.4 0.0 all-gather.15.cloned.1.call-done
  154.4 2.6 fusion.3
  157.0 0.0 copy-start.2
  157.1 61.3 %all-gather.9.cloned.1.call-done = bf16[1024,6144]{1,0:T(8,128)(2,1)} async-done(((bf16[32,6144]{1,0:T(8,128)(2,1)}), bf16[1024,6144]{1,0:T(8,128)(2,1)}) %all-gather.9.cloned.1.call-update) | async-done | bytes 12582928 | tf_op jit(solution)/shard_map/all_gather | solution.py:12
  218.4 0.0 copy-done.12
  218.4 6.2 fusion.10
  224.6 0.0 copy-done.2
  224.6 7.3 %multiply_multiply_fusion = f32[768,1024]{1,0:T(8,128)} fusion(f32[768,1024]{1,0:T(8,128)S(1)} %fusion.10, bf16[1024,6144]{1,0:T(8,128)(2,1)} %all-gather.9.cloned.1.call-done, f32[1024]{0:T(1024)S(1)} %bitcast.78, f32[1024]{0:T(1024)S(1)} %bitcast.79, bf16[1,768,2048]{2,1,0:T(8,128)(2,1)S(1)} %copy-done.2, f32[2048]{0:T(1024)S(1)} %copy-done.12, ...), kind=kOutput, calls=%fused_computation.42 | convolution fusion | flops 3229876224 | bytes 13650944 | tf_op jit(solution)/shard_map/dot_general | solution.py:73
  231.9 0.0 all-to-all-done
  231.9 15.2 %multiply_convert_fusion.1 = bf16[768,2048]{1,0:T(8,128)(2,1)} fusion(bf16[1024,2048]{0,1:T(8,128)(2,1)} %bitcast.12, f32[2048]{0:T(1024)S(1)} %bitcast.73, f32[768,1024]{1,0:T(8,128)} %multiply_multiply_fusion, bf16[1024,6144]{1,0:T(8,128)(2,1)} %all-gather.9.cloned.1.call-done, f32[1024]{0:T(1024)S(1)} %bitcast.76, f32[1024]{0:T(1024)S(1)} %bitcast.77, ...), kind=kOutput, calls=%fused_computation.13 | convolution fusion | flops 6458179584 | bytes 17861632 | tf_op jit(solution)/shard_map/dot_general | solution.py:83
  247.2 2.3 copy.26
  249.4 22.6 %all_to_all.15 = bf16[2,768,1024]{2,1,0:T(8,128)(2,1)S(1)} all-to-all(bf16[2,768,1024]{2,1,0:T(8,128)(2,1)S(1)} %bitcast.68), channel_id=1, replica_groups=mesh['rep'=2,'fs'=32,'tp'=2] {'tp'}, dimensions={0} | all-to-all | bytes 6291456 | tf_op jit(solution)/shard_map/all_to_all | solution.py:28
  272.0 0.7 convert_reduce_fusion.1
  272.7 0.7 copy-done
  273.4 1.7 fusion.26
  275.1 0.0 all-gather.11.cloned.1.call-update
  275.2 0.0 all-gather.13.cloned.1.call-start
  275.2 0.0 copy-done.5
  275.2 0.7 convert_element_type.94
  275.9 0.0 all-gather.13.cloned.1.call-update
  275.9 0.0 copy-done.7
  276.0 0.0 copy-start.13
  276.0 115.6 %all-gather.17.cloned.1.call-done = bf16[32,44,4096]{2,1,0:T(8,128)(2,1)} async-done(((bf16[1,44,4096]{2,1,0:T(8,128)(2,1)}), bf16[32,44,4096]{2,1,0:T(8,128)(2,1)}) %all-gather.17.cloned.1.call-update) | async-done | bytes 11534352 | tf_op jit(solution)/shard_map/all_gather | solution.py:12
  391.6 14.3 %reshape.54 = bf16[1408,4096]{1,0:T(8,128)(2,1)} reshape(bf16[32,44,4096]{2,1,0:T(8,128)(2,1)} %all-gather.17.cloned.1.call-done) | data formatting | bytes 23068672
  405.9 19.0 %all-gather.11.cloned.1.call-done = bf16[768,2048]{1,0:T(8,128)(2,1)} async-done(((bf16[768,1024]{1,0:T(8,128)(2,1)}), bf16[768,2048]{1,0:T(8,128)(2,1)}) %all-gather.11.cloned.1.call-update) | async-done | bytes 3145744 | tf_op jit(solution)/shard_map/all_gather | solution.py:88
  425.0 2.6 fusion
  427.5 0.0 copy-done.13
  427.5 9.9 %fusion.6 = f32[768,1408]{1,0:T(8,128)} fusion(bf16[1408,4096]{1,0:T(8,128)(2,1)} %reshape.54, bf16[768,2048]{1,0:T(8,128)(2,1)} %all-gather.11.cloned.1.call-done, f32[2048]{0:T(1024)S(1)} %copy-done.13, f32[768]{0:T(1024)S(1)} %add_rsqrt_fusion), kind=kOutput, calls=%fused_computation.14 | convolution fusion | flops 4435476480 | bytes 13249536 | tf_op jit(solution)/shard_map/dot_general | solution.py:94
  437.4 130.3 %all-gather.13.cloned.1.call-done = bf16[1408,2048]{0,1:T(8,128)(2,1)} async-done(((bf16[1408,64]{0,1:T(8,128)(2,1)}), bf16[1408,2048]{0,1:T(8,128)(2,1)}) %all-gather.13.cloned.1.call-update) | async-done | bytes 5767184 | tf_op jit(solution)/shard_map/all_gather | solution.py:100
  567.7 17.4 %multiply_convert_fusion = bf16[768,2048]{1,0:T(8,128)(2,1)} fusion(bf16[1408,2048]{0,1:T(8,128)(2,1)} %all-gather.13.cloned.1.call-done, f32[2048]{0:T(1024)S(1)} %bitcast.72, f32[768,1408]{1,0:T(8,128)} %fusion.6, bf16[1408,4096]{1,0:T(8,128)(2,1)} %reshape.54, f32[1408]{0:T(1024)S(1)} %get-tuple-element.6, f32[1408]{0:T(1024)S(1)} %get-tuple-element.5, ...), kind=kOutput, calls=%fused_computation.11 | convolution fusion | flops 8876457984 | bytes 22181888 | tf_op jit(solution)/shard_map/dot_general | solution.py:98
  585.1 2.3 copy.25
  587.4 26.0 %all_to_all.16 = bf16[2,768,1024]{2,1,0:T(8,128)(2,1)S(1)} all-to-all(bf16[2,768,1024]{2,1,0:T(8,128)(2,1)S(1)} %bitcast.69), channel_id=1, replica_groups=mesh['rep'=2,'fs'=32,'tp'=2] {'tp'}, dimensions={0} | all-to-all | bytes 6291456 | tf_op jit(solution)/shard_map/all_to_all | solution.py:28
  613.4 0.7 convert_reduce_fusion
  614.1 0.7 copy-done.1
  614.8 2.1 fusion.27
  (15 shorter events, 0.2 us)
Async XLA Ops:
  6.5 3.7 copy-start.4
  6.5 3.7 copy-start.3
  6.5 4.6 copy-start.6
  6.5 147.9 %all-gather.15.cloned.1.call-start = ((), (), s32[]{:S(2)}) async-start(), calls=%async_computation.6 | async-start | bytes 4718592 | tf_op jit(solution)/shard_map/all_gather | solution.py:63
  7.3 211.1 %all-gather.9.cloned.1.call-start = ((), (), s32[]{:S(2)}) async-start(), calls=%async_computation.3 | async-start | bytes 12976128 | tf_op jit(solution)/shard_map/all_gather | solution.py:12
  10.1 381.5 %all-gather.17.cloned.1.call-start = ((), (), s32[]{:S(2)}) async-start(), calls=%async_computation.7 | async-start | bytes 12976128 | tf_op jit(solution)/shard_map/all_gather | solution.py:12
  13.6 9.6 %copy-start.10 = (f32[64]{0:T(128)S(1)}, f32[64]{0:T(128)}, u32[]{:S(2)}) copy-start(f32[64]{0:T(128)} %param.29) | copy-start | bytes 772
  13.6 9.6 %copy-start.11 = (f32[64]{0:T(128)S(1)}, f32[64]{0:T(128)}, u32[]{:S(2)}) copy-start(f32[64]{0:T(128)} %param.24) | copy-start | bytes 772
  13.6 140.7 %copy-start.8 = (f32[3,1024]{1,0:T(4,128)S(1)}, f32[3,1024]{1,0:T(4,128)}, u32[]{:S(2)}) copy-start(f32[3,1024]{1,0:T(4,128)} %param.21) | copy-start | bytes 36868
  13.6 140.7 %copy-start.9 = (f32[3,1024]{1,0:T(4,128)S(1)}, f32[3,1024]{1,0:T(4,128)}, u32[]{:S(2)}) copy-start(f32[3,1024]{1,0:T(4,128)} %param.22) | copy-start | bytes 36868
  13.6 218.3 %all-to-all-start = ((bf16[32,1024,64]{1,2,0:T(8,128)(2,1)}), bf16[32,1024,64]{1,2,0:T(8,128)(2,1)}, u32[]{:S(2)}, u32[]{:S(2)}) async-start(bf16[32,1024,64]{1,2,0:T(8,128)(2,1)} %stack.2), calls=%async_computation | async-start | bytes 8388608 | tf_op jit(solution)/shard_map/all_to_all | solution.py:58
  23.1 195.3 %copy-start.12 = (f32[2048]{0:T(1024)S(1)}, f32[2048]{0:T(1024)}, u32[]{:S(2)}) copy-start(f32[2048]{0:T(1024)} %param.16) | copy-start | bytes 24580
  23.1 401.8 %all-gather.11.cloned.1.call-start = ((), (), s32[]{:S(2)}) async-start(), calls=%async_computation.4 | async-start | bytes 4718592 | tf_op jit(solution)/shard_map/all_gather | solution.py:88
  157.0 67.6 %copy-start.2 = (bf16[1,768,2048]{2,1,0:T(8,128)(2,1)S(1)}, bf16[1,768,2048]{2,1,0:T(8,128)(2,1)}, u32[]{:S(2)}) copy-start(bf16[1,768,2048]{2,1,0:T(8,128)(2,1)} %all-gather.15.cloned.1.call-done) | copy-start | bytes 9437188
  272.0 1.4 copy-start
  273.4 1.8 copy-start.5
  273.4 2.5 copy-start.7
  275.2 292.6 %all-gather.13.cloned.1.call-start = ((), (), s32[]{:S(2)}) async-start(), calls=%async_computation.5 | async-start | bytes 5947392 | tf_op jit(solution)/shard_map/all_gather | solution.py:100
  276.0 151.5 %copy-start.13 = (f32[2048]{0:T(1024)S(1)}, f32[2048]{0:T(1024)}, u32[]{:S(2)}) copy-start(f32[2048]{0:T(1024)} %param.17) | copy-start | bytes 24580
  613.4 1.4 copy-start.1
Sparse Core Ops, SparseCore 0:
  9.0 18.4 all-gather.14
  29.1 189.2 all-gather.8
  220.0 171.5 all-gather.16
  393.1 31.7 all-gather.10
  426.4 141.2 all-gather.12
